TPU v7x, 32 devices: a whole 2x2x4 slice. The times are simulated.
32 devices in a mesh: fs: 8 (over z, y), tp: 4 (over x, core).
Axes of the slice: x: 2, y: 2, z: 4, core: 2. Of those that a mesh axis runs over, the one named last changes fastest.
Arguments:
- tokens: bfloat16 [16, 384, 2048], P('fs', None, 'tp'), may hold values from -34 to 34
- mix_gain: float32 [2048], replicated, may hold values from 0.1 to 1.9
- w_bgate: float32 [2048, 2048], P('fs', 'tp'), may hold values from -0.125 to 0.125
- w_cgate: float32 [2048, 2048], P('fs', 'tp'), may hold values from -0.125 to 0.125
- w_value: float32 [2048, 2048], P('fs', 'tp'), may hold values from -0.125 to 0.125
- in_scale: float32 [3, 2048], P(None, 'tp'), may hold values from 0.5 to 2
- mix_taps: float32 [3, 2048], P(None, 'tp'), may hold values from -3.5 to 3.5
- w_mixout: float32 [2048, 2048], P('tp', 'fs'), may hold values from -0.125 to 0.125
- mixout_scale: float32 [1, 2048], P(None, 'fs'), may hold values from 0.5 to 2
- ffn_gain: float32 [2048], replicated, may hold values from 0.1 to 1.9
- w_upgate: float32 [2048, 5632], P('fs', 'tp'), may hold values from -0.125 to 0.125
- w_upval: float32 [2048, 5632], P('fs', 'tp'), may hold values from -0.125 to 0.125
- up_scale: float32 [2, 5632], P(None, 'tp'), may hold values from 0.5 to 2
- ffn_taps: float32 [2, 3, 5632], P(None, None, 'tp'), may hold values from -3.5 to 3.5
- w_down: float32 [5632, 2048], P('tp', 'fs'), may hold values from -0.078125 to 0.078125
- down_scale: float32 [1, 2048], P(None, 'fs'), may hold values from 0.5 to 2
Outputs:
- layer_out: bfloat16 [16, 384, 2048], P('fs', None, 'tp')
All inputs are finite; a program needn't handle non-finite values.
Results may differ from a plain program's by a relative error of at most 0.015.
Values may be sent and summed in bfloat16 or wider, within the bound.
A program may use at most 64 MiB of HBM per device.

v0:
```python
import jax
import jax.numpy as jnp
from jax import lax
from jax.sharding import PartitionSpec as P

EPS = 1e-06


def causal_taps(values, taps):
    length = values.shape[1]
    kernel = taps.shape[0]
    padded = jnp.pad(values, ((0, 0), (kernel - 1, 0), (0, 0)))
    result = jnp.zeros(values.shape, jnp.float32)
    for offset in range(kernel):
        result = result + padded[:, offset : offset + length] * taps[offset]
    return result


def normed_rows(shard, gain):
    gathered = lax.all_gather(shard, "tp", axis=2, tiled=True)
    floats = gathered.astype(jnp.float32)
    factor = lax.rsqrt(jnp.mean(floats * floats, axis=-1, keepdims=True) + EPS)
    result = (floats * factor * gain).astype(jnp.bfloat16)
    return result.reshape(-1, result.shape[-1])


def scaled_columns(piece, acts, scales):
    return (jnp.dot(acts, piece, preferred_element_type=jnp.float32) * scales).astype(jnp.bfloat16)


def dot_rows(inputs, matrix):
    return jnp.dot(inputs, matrix, preferred_element_type=jnp.float32)


def on_device(
    tokens,
    mix_gain,
    w_bgate,
    w_cgate,
    w_value,
    in_scale,
    mix_taps,
    w_mixout,
    mixout_scale,
    ffn_gain,
    w_upgate,
    w_upval,
    up_scale,
    ffn_taps,
    w_down,
    down_scale,
):
    seq_count, length, own_width = tokens.shape
    row_count = seq_count * length
    ff_width = w_upgate.shape[1]
    mix_scales, down_scales = (
        lax.all_gather(mixout_scale, "fs", axis=1, tiled=True),
        lax.all_gather(down_scale, "fs", axis=1, tiled=True),
    )
    normed = normed_rows(tokens, mix_gain)
    bgate_rows = w_bgate.astype(jnp.bfloat16)
    cgate_rows = w_cgate.astype(jnp.bfloat16)
    value_rows = w_value.astype(jnp.bfloat16)
    bgate_full, cgate_full, value_full = (
        lax.all_gather(bgate_rows, "fs", axis=0, tiled=True),
        lax.all_gather(cgate_rows, "fs", axis=0, tiled=True),
        lax.all_gather(value_rows, "fs", axis=0, tiled=True),
    )
    bgate = dot_rows(normed, bgate_full)
    cgate = dot_rows(normed, cgate_full)
    value = dot_rows(normed, value_full)
    bgate = bgate * in_scale[0]
    inner = cgate * in_scale[1] * (value * in_scale[2])
    convolved = causal_taps(inner.reshape(seq_count, length, own_width), mix_taps)
    gated = (
        (bgate.reshape(seq_count, length, own_width) * convolved)
        .astype(jnp.bfloat16)
        .reshape(row_count, own_width)
    )
    mix_terms = scaled_columns(
        lax.all_gather(w_mixout.astype(jnp.bfloat16), "fs", axis=1, tiled=True),
        acts=gated,
        scales=mix_scales,
    )
    mix = lax.psum_scatter(
        mix_terms.astype(jnp.float32).astype(jnp.bfloat16), "tp", scatter_dimension=1, tiled=True
    ).astype(jnp.float32)
    resid = (tokens.reshape(row_count, own_width).astype(jnp.float32) + mix).astype(jnp.bfloat16)
    normed_ffn = normed_rows(resid.reshape(seq_count, length, own_width), ffn_gain)
    upgate_rows = w_upgate.astype(jnp.bfloat16)
    upval_rows = w_upval.astype(jnp.bfloat16)
    upgate_full, upval_full = (
        lax.all_gather(upgate_rows, "fs", axis=0, tiled=True),
        lax.all_gather(upval_rows, "fs", axis=0, tiled=True),
    )
    gate_pre = dot_rows(normed_ffn, upgate_full)
    val_pre = dot_rows(normed_ffn, upval_full)
    gate_pre = (gate_pre * up_scale[0]).reshape(seq_count, length, ff_width)
    val_pre = (val_pre * up_scale[1]).reshape(seq_count, length, ff_width)
    gate_conv = causal_taps(gate_pre, ffn_taps[0])
    val_conv = causal_taps(val_pre, ffn_taps[1])
    active = (jax.nn.silu(gate_conv) * val_conv).astype(jnp.bfloat16).reshape(row_count, ff_width)
    down_terms = scaled_columns(
        lax.all_gather(w_down.astype(jnp.bfloat16), "fs", axis=1, tiled=True),
        acts=active,
        scales=down_scales,
    )
    ffn = lax.psum_scatter(
        down_terms.astype(jnp.float32).astype(jnp.bfloat16), "tp", scatter_dimension=1, tiled=True
    ).astype(jnp.float32)
    layer_out = (resid.astype(jnp.float32) + ffn).astype(jnp.bfloat16)
    return layer_out.reshape(seq_count, length, own_width)


def solution(mesh):
    in_specs = (
        P("fs", None, "tp"),
        P(),
        P("fs", "tp"),
        P("fs", "tp"),
        P("fs", "tp"),
        P(None, "tp"),
        P(None, "tp"),
        P("tp", "fs"),
        P(None, "fs"),
        P(),
        P("fs", "tp"),
        P("fs", "tp"),
        P(None, "tp"),
        P(None, None, "tp"),
        P("tp", "fs"),
        P(None, "fs"),
    )
    out_specs = P("fs", None, "tp")
    return jax.shard_map(
        on_device, mesh=mesh, in_specs=in_specs, out_specs=out_specs, check_vma=False
    )
```

profile of v0, /device:TPU:3, one launch (start us, length us, event | category | flops | bytes accessed | tf_op | source)
XLA Modules:
  0.0 645.5 jit_solution(3432775690748300815)
XLA Ops:
  7.3 1.8 convert_element_type.80
  9.2 1.8 convert_element_type.79
  12.7 17.1 %all_gather.38 = f32[1,2048]{1,0:T(1,128)S(1)} all-gather(f32[1,256]{1,0:T(1,128)S(1)} %copy-done.17), channel_id=1, replica_groups=mesh['fs'=8,'tp'=4] {'fs'}, dimensions={1}, use_global_device_ids=true | all-gather | bytes 9216 | tf_op jit(solution)/shard_map/all_gather | solution.py:57
  29.8 8.2 %all-gather.10.cloned.1.call-done = bf16[2,384,2048]{2,1,0:T(8,128)(2,1)} async-done(((bf16[2,384,512]{2,1,0:T(8,128)(2,1)}), bf16[2,384,2048]{2,1,0:T(8,128)(2,1)}) %all-gather.10.cloned.1.call-update) | async-done | bytes 3145744 | tf_op jit(solution)/shard_map/all_gather | solution.py:20
  38.0 2.7 fusion
  40.8 0.8 fusion.2
  41.6 46.4 %all-gather.14.cloned.1.call-done = bf16[2048,512]{1,0:T(8,128)(2,1)} async-done(((bf16[256,512]{1,0:T(8,128)(2,1)}), bf16[2048,512]{1,0:T(8,128)(2,1)}) %all-gather.14.cloned.1.call-update) | async-done | bytes 2097168 | tf_op jit(solution)/shard_map/all_gather | solution.py:66
  88.0 4.5 fusion.9
  92.6 45.2 %all-gather.12.cloned.1.call-done = bf16[2048,512]{1,0:T(8,128)(2,1)} async-done(((bf16[256,512]{1,0:T(8,128)(2,1)}), bf16[2048,512]{1,0:T(8,128)(2,1)}) %all-gather.12.cloned.1.call-update) | async-done | bytes 2097168 | tf_op jit(solution)/shard_map/all_gather | solution.py:65
  137.8 4.5 convolution_multiply_fusion.2
  142.3 45.1 %all-gather.16.cloned.1.call-done = bf16[2048,512]{1,0:T(8,128)(2,1)} async-done(((bf16[256,512]{1,0:T(8,128)(2,1)}), bf16[2048,512]{1,0:T(8,128)(2,1)}) %all-gather.16.cloned.1.call-update) | async-done | bytes 2097168 | tf_op jit(solution)/shard_map/all_gather | solution.py:67
  187.4 3.9 multiply_multiply_fusion
  191.9 47.5 %all-gather.18.cloned.1.call-done = bf16[512,2048]{1,0:T(8,128)(2,1)} async-done(((bf16[512,256]{1,0:T(8,128)(2,1)}), bf16[512,2048]{1,0:T(8,128)(2,1)}) %all-gather.18.cloned.1.call-update) | async-done | bytes 2097168 | tf_op jit(solution)/shard_map/all_gather | solution.py:81
  239.4 5.0 multiply_convert_fusion.1
  244.6 35.6 %reduce-scatter.3.cloned.1.call-done = bf16[768,512]{1,0:T(8,128)(2,1)} async-done(((bf16[768,2048]{1,0:T(8,128)(2,1)}), bf16[768,512]{1,0:T(8,128)(2,1)}) %reduce-scatter.3.cloned.1.call-update) | async-done | bytes 786448 | tf_op jit(solution)/shard_map/reduce_scatter | solution.py:85
  280.2 2.2 fusion.6
  282.5 0.9 convert_element_type.90
  284.0 0.9 convert_element_type.91
  285.1 1.0 convert_element_type.93
  286.1 17.0 %all_gather.43 = f32[1,2048]{1,0:T(1,128)S(1)} all-gather(f32[1,256]{1,0:T(1,128)S(1)} %copy-done.18), channel_id=1, replica_groups=mesh['fs'=8,'tp'=4] {'fs'}, dimensions={1}, use_global_device_ids=true | all-gather | bytes 9216 | tf_op jit(solution)/shard_map/all_gather | solution.py:58
  303.2 8.2 %all-gather.20.cloned.1.call-done = bf16[2,384,2048]{2,1,0:T(8,128)(2,1)} async-done(((bf16[2,384,512]{2,1,0:T(8,128)(2,1)}), bf16[2,384,2048]{2,1,0:T(8,128)(2,1)}) %all-gather.20.cloned.1.call-update) | async-done | bytes 3145744 | tf_op jit(solution)/shard_map/all_gather | solution.py:20
  311.5 2.7 fusion.3
  314.3 0.8 fusion.5
  315.1 90.1 %all-gather.22.cloned.1.call-done = bf16[2048,1408]{1,0:T(8,128)(2,1)} async-done(((bf16[256,1408]{1,0:T(8,128)(2,1)}), bf16[2048,1408]{1,0:T(8,128)(2,1)}) %all-gather.22.cloned.1.call-update) | async-done | bytes 5767184 | tf_op jit(solution)/shard_map/all_gather | solution.py:93
  405.2 9.2 %convolution_multiply_fusion.1 = f32[768,1408]{1,0:T(8,128)} fusion(bf16[768,2048]{1,0:T(8,128)(2,1)S(1)} %bitcast.41, bf16[2048,1408]{1,0:T(8,128)(2,1)} %all-gather.22.cloned.1.call-done, f32[1408]{0:T(1024)S(1)} %get-tuple-element.11), kind=kOutput, calls=%fused_computation.14 | convolution fusion | flops 4430266368 | bytes 13243904 | tf_op jit(solution)/shard_map/dot_general | solution.py:32
  414.4 83.5 %all-gather.24.cloned.1.call-done = bf16[2048,1408]{1,0:T(8,128)(2,1)} async-done(((bf16[256,1408]{1,0:T(8,128)(2,1)}), bf16[2048,1408]{1,0:T(8,128)(2,1)}) %all-gather.24.cloned.1.call-update) | async-done | bytes 5767184 | tf_op jit(solution)/shard_map/all_gather | solution.py:94
  497.9 7.6 %convolution_multiply_fusion = f32[768,1408]{1,0:T(8,128)S(1)} fusion(bf16[768,2048]{1,0:T(8,128)(2,1)S(1)} %bitcast.42, bf16[2048,1408]{1,0:T(8,128)(2,1)} %all-gather.24.cloned.1.call-done, f32[1408]{0:T(1024)S(1)} %get-tuple-element.12), kind=kOutput, calls=%fused_computation.13 | convolution fusion | flops 4430266368 | bytes 13243904 | tf_op jit(solution)/shard_map/dot_general | solution.py:32
  505.5 3.6 multiply_convert_fusion.2
  509.1 82.9 %all-gather.26.cloned.1.call-done = bf16[1408,2048]{1,0:T(8,128)(2,1)} async-done(((bf16[1408,256]{1,0:T(8,128)(2,1)}), bf16[1408,2048]{1,0:T(8,128)(2,1)}) %all-gather.26.cloned.1.call-update) | async-done | bytes 5767184 | tf_op jit(solution)/shard_map/all_gather | solution.py:104
  592.0 9.1 %multiply_convert_fusion = bf16[768,2048]{1,0:T(8,128)(2,1)} fusion(bf16[768,1408]{1,0:T(8,128)(2,1)S(1)} %bitcast.43, bf16[1408,2048]{1,0:T(8,128)(2,1)} %all-gather.26.cloned.1.call-done, f32[2048]{0:T(1024)S(1)} %bitcast.51), kind=kOutput, calls=%fused_computation.10 | convolution fusion | flops 4432330752 | bytes 11083776 | tf_op jit(solution)/shard_map/dot_general | solution.py:28
  601.1 35.6 %reduce-scatter.5.cloned.1.call-done = bf16[768,512]{1,0:T(8,128)(2,1)} async-done(((bf16[768,2048]{1,0:T(8,128)(2,1)}), bf16[768,512]{1,0:T(8,128)(2,1)}) %reduce-scatter.5.cloned.1.call-update) | async-done | bytes 786448 | tf_op jit(solution)/shard_map/reduce_scatter | solution.py:108
  636.7 2.2 add_convert_fusion
  (69 shorter events, 4.2 us)
Async XLA Ops:
  6.5 4.5 copy-start.9
  6.5 5.3 copy-start.10
  6.5 6.1 copy-start.17
  6.5 23.2 %copy-start.15 = (f32[3,512]{1,0:T(4,128)S(1)}, f32[3,512]{1,0:T(4,128)}, u32[]{:S(2)}) copy-start(f32[3,512]{1,0:T(4,128)} %param.21) | copy-start | bytes 18436
  6.5 23.2 %copy-start.16 = (f32[3,512]{1,0:T(4,128)S(1)}, f32[3,512]{1,0:T(4,128)}, u32[]{:S(2)}) copy-start(f32[3,512]{1,0:T(4,128)} %param.22) | copy-start | bytes 18436
  6.5 31.4 %all-gather.10.cloned.1.call-start = ((), (), s32[]{:S(2)}) async-start(), calls=%async_computation.2 | async-start | bytes 3932160 | tf_op jit(solution)/shard_map/all_gather | solution.py:20
  7.3 80.7 %all-gather.14.cloned.1.call-start = ((), (), s32[]{:S(2)}) async-start(), calls=%async_computation.4 | async-start | bytes 2359296 | tf_op jit(solution)/shard_map/all_gather | solution.py:66
  9.1 31.6 %copy-start.13 = (f32[2048]{0:T(1024)S(1)}, f32[2048]{0:T(1024)}, u32[]{:S(2)}) copy-start(f32[2048]{0:T(1024)} %param.17) | copy-start | bytes 24580
  9.1 128.7 %all-gather.12.cloned.1.call-start = ((), (), s32[]{:S(2)}) async-start(), calls=%async_computation.3 | async-start | bytes 2359296 | tf_op jit(solution)/shard_map/all_gather | solution.py:65
  11.0 176.4 %all-gather.16.cloned.1.call-start = ((), (), s32[]{:S(2)}) async-start(), calls=%async_computation.5 | async-start | bytes 2359296 | tf_op jit(solution)/shard_map/all_gather | solution.py:67
  11.8 227.6 %all-gather.18.cloned.1.call-start = ((), (), s32[]{:S(2)}) async-start(), calls=%async_computation.6 | async-start | bytes 2359296 | tf_op jit(solution)/shard_map/all_gather | solution.py:81
  12.6 267.6 %reduce-scatter.3.cloned.1.call-start = ((), (), s32[]{:S(2)}) async-start(), calls=%async_computation.7 | async-start | bytes 3932160 | tf_op jit(solution)/shard_map/reduce_scatter | solution.py:85
  38.0 2.8 copy-start
  187.4 4.0 copy-start.5
  244.5 35.7 %copy-start.4 = (bf16[2,384,512]{2,1,0:T(8,128)(2,1)S(1)}, bf16[2,384,512]{2,1,0:T(8,128)(2,1)}, u32[]{:S(2)}) copy-start(bf16[2,384,512]{2,1,0:T(8,128)(2,1)} %param.16) | copy-start | bytes 2359300
  244.5 38.0 %copy-start.6 = (f32[256,1408]{1,0:T(8,128)S(1)}, f32[256,1408]{1,0:T(8,128)}, u32[]{:S(2)}) copy-start(f32[256,1408]{1,0:T(8,128)} %param.26) | copy-start | bytes 4325380
  244.5 67.0 %all-gather.20.cloned.1.call-start = ((), (), s32[]{:S(2)}) async-start(), calls=%async_computation.8 | async-start | bytes 3932160 | tf_op jit(solution)/shard_map/all_gather | solution.py:20
  282.4 1.6 copy-start.7
  282.4 122.8 %all-gather.22.cloned.1.call-start = ((), (), s32[]{:S(2)}) async-start(), calls=%async_computation.9 | async-start | bytes 6488064 | tf_op jit(solution)/shard_map/all_gather | solution.py:93
  283.4 1.6 copy-start.8
  283.4 2.7 copy-start.18
  283.4 19.7 %copy-start.12 = (f32[2,1408]{1,0:T(2,128)S(1)}, f32[2,1408]{1,0:T(2,128)}, u32[]{:S(2)}) copy-start(f32[2,1408]{1,0:T(2,128)} %param.28) | copy-start | bytes 33796
  283.4 19.7 %copy-start.11 = (f32[2,3,1408]{2,0,1:T(2,128)S(1)}, f32[2,3,1408]{2,0,1:T(2,128)}, u32[]{:S(2)}) copy-start(f32[2,3,1408]{2,0,1:T(2,128)} %param.29) | copy-start | bytes 101380
  283.5 214.5 %all-gather.24.cloned.1.call-start = ((), (), s32[]{:S(2)}) async-start(), calls=%async_computation.10 | async-start | bytes 6488064 | tf_op jit(solution)/shard_map/all_gather | solution.py:94
  285.0 29.2 %copy-start.14 = (f32[2048]{0:T(1024)S(1)}, f32[2048]{0:T(1024)}, u32[]{:S(2)}) copy-start(f32[2048]{0:T(1024)} %param.25) | copy-start | bytes 24580
  285.0 307.0 %all-gather.26.cloned.1.call-start = ((), (), s32[]{:S(2)}) async-start(), calls=%async_computation.11 | async-start | bytes 6488064 | tf_op jit(solution)/shard_map/all_gather | solution.py:104
  286.0 350.7 %reduce-scatter.5.cloned.1.call-start = ((), (), s32[]{:S(2)}) async-start(), calls=%async_computation.12 | async-start | bytes 3932160 | tf_op jit(solution)/shard_map/reduce_scatter | solution.py:108
  311.5 2.8 copy-start.1
  497.9 7.6 %copy-start.3 = (f32[768,1408]{1,0:T(8,128)S(1)}, f32[768,1408]{1,0:T(8,128)}, u32[]{:S(2)}) copy-start(f32[768,1408]{1,0:T(8,128)} %convolution_multiply_fusion.1) | copy-start | bytes 12976132
  601.1 35.7 %copy-start.2 = (bf16[768,512]{1,0:T(8,128)(2,1)S(1)}, bf16[768,512]{1,0:T(8,128)(2,1)}, u32[]{:S(2)}) copy-start(bf16[768,512]{1,0:T(8,128)(2,1)} %fusion.6) | copy-start | bytes 2359300
Sparse Core Ops, SparseCore 0:
  8.9 28.9 all-gather.9
  40.1 47.8 all-gather.13
  90.1 47.6 all-gather.11
  139.8 47.6 all-gather.15
  189.3 50.0 all-gather.17
  244.6 35.4 reduce-scatter.2
  282.5 28.8 all-gather.19
  313.6 91.4 all-gather.21
  407.4 90.4 all-gather.23
  499.8 92.1 all-gather.25
  601.2 35.4 reduce-scatter.4
where the time goes:
time: 649 us; the launch traced here: 645 us
  waiting for transfers between devices  529 us (82%)
  matrix products  44 us (7%)
  blocking collectives  34.1 us (5%)
  other arithmetic  23.4 us (4%)
  between operations  13.4 us (2%)
    all_gather x1, waiting for transfers between devices, on_device(): lax.all_gather(upgate_rows, 'fs', axis=0, tiled=True)  90.1 us
    all_gather x1, waiting for transfers between devices, on_device(): lax.all_gather(upval_rows, 'fs', axis=0, tiled=True)  83.5 us
    all_gather x1, waiting for transfers between devices, on_device(): lax.all_gather(w_down.astype(jnp.bfloat16), 'fs', axis=1, tiled=True)  82.9 us
    all_gather x1, waiting for transfers between devices, on_device(): lax.all_gather(w_mixout.astype(jnp.bfloat16), 'fs', axis=1, tiled=True)  47.5 us
    all_gather x1, waiting for transfers between devices, on_device(): lax.all_gather(cgate_rows, 'fs', axis=0, tiled=True)  46.4 us
    all_gather x1, waiting for transfers between devices, on_device(): lax.all_gather(bgate_rows, 'fs', axis=0, tiled=True)  45.2 us
    all_gather x1, waiting for transfers between devices, on_device(): lax.all_gather(value_rows, 'fs', axis=0, tiled=True)  45.1 us
    reduce_scatter x1, waiting for transfers between devices, on_device(): lax.psum_scatter(down_terms.astype(jnp.float32).astype(jnp.bfloat16), 'tp...  35.6 us
  transfers between devices with their start and end apart: 11, of which 11 were waited for; matrix products, arithmetic and copies ran while one was open for 8% of the time, Pallas kernels for 0%

commit v1 on v0

v1 whole, which is shorter than its diff:
```python
import functools

import jax
import jax.numpy as jnp
from jax import lax
from jax.experimental import pallas as pl
from jax.experimental.pallas import tpu as pltpu
from jax.sharding import PartitionSpec as P

EPS = 1e-06
MESH = pl.DeviceIdType.MESH
F32 = jnp.float32
BF16 = jnp.bfloat16
S, A, B, C, D = range(5)


def shifted(values, by):
    rows = lax.broadcasted_iota(jnp.int32, values.shape, 0)
    return jnp.where(rows >= by, pltpu.roll(values, by, 0), 0.0)


def causal_taps(values, taps):
    return shifted(values, 2) * taps[0:1] + shifted(values, 1) * taps[1:2] + values * taps[2:3]


def layer_kernel(
    n, n_tp, seqs, tok, gain1, gain2, iscale, mtaps, uscale, ftaps, w_s, w_a, w_b, w_c, w_d, out,
    buf_s, buf_a, buf_b, buf_c, buf_d, xg, rg, normed, gated, active,
    parts_m, recv_m, parts_d, recv_d,
    ring_send, ring_recv, tok_send, tok_recv, mix_send, mix_recv, res_send, res_recv,
    down_send, down_recv, local_sem,
):
    fs, me = lax.axis_index("fs"), lax.axis_index("tp")
    rows, own = tok.shape
    length = rows // seqs
    bpo = n // n_tp
    bw = own // bpo
    width = own * n_tp
    weights = (w_s, w_a, w_b, w_c, w_d)
    bufs = (buf_s, buf_a, buf_b, buf_c, buf_d)
    hi, lo = n // 2, n - 1 - n // 2

    odd = fs % 2
    pos = (1 - odd) * (fs // 2) + odd * (n - 1 - fs // 2)

    def member(q):
        q = (q + 2 * n) % n
        back = q // (n // 2)
        return (1 - back) * (2 * q) + back * (2 * (n - 1 - q) + 1)

    def hops(h, d):
        return hi if h == d else lo

    def ring(g, h, d, k):
        sign = 1 - 2 * d
        owner = member(pos - sign * (k - 1))
        half = weights[g].shape[0] // 2
        part = pl.ds(h * half, half)
        dst = bufs[g].at[owner, part]
        return pltpu.make_async_remote_copy(
            src_ref=weights[g].at[part] if k == 1 else dst,
            dst_ref=dst,
            send_sem=ring_send.at[g, h, d, k - 1],
            recv_sem=ring_recv.at[g, h, d, k - 1],
            device_id={"fs": member(pos + sign)},
            device_id_type=MESH,
        )

    def begin(g, halves=(0, 1)):
        for h in halves:
            for d in (0, 1):
                ring(g, h, d, 1).start()

    def arrive(g, k, halves=(0, 1)):
        for h in halves:
            for d in (0, 1):
                if k <= hops(h, d):
                    ring(g, h, d, k).wait_recv()
                    if k < hops(h, d):
                        ring(g, h, d, k + 1).start()

    def to_peer(src, dst, send, recv, r):
        return pltpu.make_async_remote_copy(
            src_ref=src, dst_ref=dst, send_sem=send, recv_sem=recv,
            device_id={"tp": (me + r) % n_tp}, device_id_type=MESH,
        )

    barrier = pltpu.get_barrier_semaphore()
    for sign in (1, -1):
        pl.semaphore_signal(
            barrier, inc=1, device_id={"fs": member(pos + sign)}, device_id_type=MESH
        )
    for r in range(1, n_tp):
        pl.semaphore_signal(
            barrier, inc=1, device_id={"tp": (me + r) % n_tp}, device_id_type=MESH
        )
    pl.semaphore_wait(barrier, 1 + n_tp)

    begin(S)
    begin(A)
    tok_copies = [
        to_peer(tok, xg.at[me], tok_send.at[r - 1], tok_recv.at[r - 1], r) for r in range(1, n_tp)
    ]
    for copy in tok_copies:
        copy.start()
    locals_ = [
        pltpu.make_async_copy(weights[g], bufs[g].at[fs], local_sem.at[g]) for g in range(5)
    ]
    for copy in locals_:
        copy.start()
    xg[me] = tok[...]

    def normalize(source, gain):
        tile = 32

        def step(i, carry):
            at = pl.ds(pl.multiple_of(i * tile, tile), tile)
            squares = jnp.zeros((tile, 1), F32)
            for t in range(n_tp):
                piece = source[t, at, :].astype(F32)
                squares = squares + jnp.sum(piece * piece, axis=-1, keepdims=True)
            factor = lax.rsqrt(squares * (1.0 / width) + EPS)
            for t in range(n_tp):
                cols = slice(t * own, (t + 1) * own)
                piece = source[t, at, :].astype(F32)
                normed[at, cols] = (piece * factor * gain[:, cols]).astype(BF16)
            return carry

        lax.fori_loop(0, rows // tile, step, 0)

    arrive(S, 1)
    arrive(A, 1)
    for k in range(2, hi + 1):
        arrive(S, k)
    for k in range(2, hi):
        arrive(A, k)
    begin(B)
    begin(C, (0,))
    for copy in tok_copies:
        copy.wait_recv()
    normalize(xg, gain1)
    arrive(A, hi)
    for copy in locals_:
        copy.wait()

    mixed = min(256, own)

    def mixer(s):
        lines = slice(s * length, (s + 1) * length)

        def step(j, carry):
            def product(i):
                at = pl.ds(pl.multiple_of(i * own + j * mixed, 128), mixed)
                matrix = buf_a[:, :, at].reshape(width, mixed)
                return jnp.dot(normed[lines, :], matrix, preferred_element_type=F32)

            at = pl.ds(pl.multiple_of(j * mixed, 128), mixed)
            scales = iscale[:, at]
            inner = (product(1) * scales[1:2]) * (product(2) * scales[2:3])
            convolved = causal_taps(inner, mtaps[:, at])
            gated[lines, at] = (product(0) * scales[0:1] * convolved).astype(BF16)
            return carry

        lax.fori_loop(0, own // mixed, step, 0)

    for s in range(seqs):
        mixer(s)
        if s == 0:
            arrive(B, 1)
    begin(C, (1,))
    for k in range(2, hi + 1):
        arrive(B, k)

    mix_copies = []
    for r in list(range(1, n_tp)) + [0]:
        for b in range(bpo):
            owner = (me + r) % n_tp * bpo + b
            for s in range(seqs):
                lines = slice(s * length, (s + 1) * length)
                part = jnp.dot(gated[lines, :], buf_b[owner], preferred_element_type=F32)
                parts_m[r * bpo + b, lines, :] = (part * buf_s[owner, 0:1, :]).astype(BF16)
            if r:
                copy = to_peer(
                    parts_m.at[r * bpo + b], recv_m.at[r - 1, b],
                    mix_send.at[r - 1, b], mix_recv.at[r - 1, b], r,
                )
                copy.start()
                mix_copies.append(copy)
    arrive(C, 1)

    for copy in mix_copies:
        copy.wait_recv()
    tile = 64

    def total_of(base, own_part, received, store):
        def step(i, carry):
            at = pl.ds(pl.multiple_of(i * tile, tile), tile)
            for b in range(bpo):
                cols = slice(b * bw, (b + 1) * bw)
                total = own_part(b, at).astype(F32)
                for r in range(1, n_tp):
                    total = total + received[r - 1, b, at, :].astype(F32)
                store(at, cols, (base(at, cols).astype(F32) + total).astype(BF16))
            return carry

        lax.fori_loop(0, rows // tile, step, 0)

    def store_resid(at, cols, values):
        rg[me, at, cols] = values

    total_of(lambda at, cols: tok[at, cols], lambda b, at: parts_m[b, at, :], recv_m, store_resid)
    res_copies = [
        to_peer(rg.at[me], rg.at[me], res_send.at[r - 1], res_recv.at[r - 1], r)
        for r in range(1, n_tp)
    ]
    for copy in res_copies:
        copy.start()
    arrive(C, 2)
    for k in range(3, hi):
        arrive(C, k)
    for copy in res_copies:
        copy.wait_recv()
    begin(D)
    normalize(rg, gain2)
    arrive(C, hi)

    tiles = buf_c.shape[2] // 256

    def up(s):
        lines = slice(s * length, (s + 1) * length)

        def step(j, carry):
            at = pl.ds(pl.multiple_of(j * 256, 256), 256)
            matrix = buf_c[:, :, at].reshape(width, 256)
            both = jnp.dot(normed[lines, :], matrix, preferred_element_type=F32) * uscale[:, at]
            both = causal_taps(both, ftaps[:, at])
            gate, val = both[:, :128], both[:, 128:]
            half = pl.ds(pl.multiple_of(j * 128, 128), 128)
            active[lines, half] = (gate / (1.0 + jnp.exp(-gate)) * val).astype(BF16)
            return carry

        lax.fori_loop(0, tiles, step, 0)

    for s in range(seqs):
        up(s)
        if s == 0:
            arrive(D, 1)

    def down(owner):
        t = owner // bpo
        r = (t - me + n_tp) % n_tp
        b = owner % bpo
        for s in range(seqs):
            lines = slice(s * length, (s + 1) * length)
            part = jnp.dot(active[lines, :], buf_d[owner], preferred_element_type=F32)
            parts_d[owner, lines, :] = (part * buf_s[owner, 1:2, :]).astype(BF16)

        @pl.when(r != 0)
        def _():
            pltpu.make_async_remote_copy(
                src_ref=parts_d.at[owner], dst_ref=recv_d.at[r - 1, b],
                send_sem=down_send.at[owner], recv_sem=down_recv.at[r - 1, b],
                device_id={"tp": t}, device_id_type=MESH,
            ).start()

    down(fs)
    for k in range(1, hi + 1):
        if k > 1:
            arrive(D, k)
        if k == 1:
            down(member(pos - 1))
            down(member(pos + 1))
        elif k > 1:
            down(member(pos - k))
            if (2 * k) % n:
                down(member(pos + k))

    ends = []
    for r in range(1, n_tp):
        for b in range(bpo):
            owner = (me + r) % n_tp * bpo + b
            ends.append(
                to_peer(
                    parts_d.at[owner], recv_d.at[r - 1, b],
                    down_send.at[owner], down_recv.at[r - 1, b], r,
                )
            )
    for copy in ends:
        copy.wait_recv()

    def store_out(at, cols, values):
        out[at, cols] = values

    total_of(
        lambda at, cols: rg[me, at, cols], lambda b, at: parts_d[me * bpo + b, at, :], recv_d,
        store_out,
    )

    for copy in tok_copies + mix_copies + res_copies + ends:
        copy.wait_send()
    for g in range(5):
        for h in (0, 1):
            for d in (0, 1):
                for k in range(1, hops(h, d) + 1):
                    ring(g, h, d, k).wait_send()


def on_device(
    n,
    n_tp,
    tokens,
    mix_gain,
    w_bgate,
    w_cgate,
    w_value,
    in_scale,
    mix_taps,
    w_mixout,
    mixout_scale,
    ffn_gain,
    w_upgate,
    w_upval,
    up_scale,
    ffn_taps,
    w_down,
    down_scale,
):
    seqs, length, own = tokens.shape
    rows = seqs * length
    width = own * n_tp
    part = w_bgate.shape[0]
    ff = w_upgate.shape[1]
    pad = -ff % 128
    ffp = ff + pad
    tiles = ffp // 128
    bw = w_mixout.shape[1]

    def interleaved(gate, val):
        pair = [jnp.pad(x, ((0, 0), (0, pad))).reshape(x.shape[0], tiles, 128) for x in (gate, val)]
        return jnp.stack(pair, axis=2).reshape(gate.shape[0], tiles * 256)

    w_s = jnp.concatenate([mixout_scale, down_scale, jnp.zeros((14, bw), F32)], axis=0)
    w_a = jnp.concatenate([w.astype(BF16) for w in (w_bgate, w_cgate, w_value)], axis=1)
    w_b = w_mixout.astype(BF16)
    w_c = interleaved(w_upgate.astype(BF16), w_upval.astype(BF16))
    w_d = jnp.pad(w_down.astype(BF16), ((0, pad), (0, 0)))
    uscale = interleaved(up_scale[0:1], up_scale[1:2])
    ftaps = interleaved(ffn_taps[0], ffn_taps[1])
    weights = (w_s, w_a, w_b, w_c, w_d)
    bpo = n // n_tp
    hi = n // 2
    vmem, dma = pltpu.VMEM, pltpu.SemaphoreType.DMA
    result = pl.pallas_call(
        functools.partial(layer_kernel, n, n_tp, seqs),
        out_shape=jax.ShapeDtypeStruct((rows, own), BF16),
        in_specs=[pl.BlockSpec(memory_space=pltpu.VMEM)] * 7
        + [pl.BlockSpec(memory_space=pl.ANY)] * 5,
        out_specs=pl.BlockSpec(memory_space=pltpu.VMEM),
        scratch_shapes=[vmem((n, *w.shape), w.dtype) for w in weights]
        + [
            vmem((n_tp, rows, own), BF16),
            vmem((n_tp, rows, own), BF16),
            vmem((rows, width), BF16),
            vmem((rows, own), BF16),
            vmem((rows, ffp), BF16),
            vmem((n, rows, bw), BF16),
            vmem((n_tp - 1, bpo, rows, bw), BF16),
            vmem((n, rows, bw), BF16),
            vmem((n_tp - 1, bpo, rows, bw), BF16),
            dma((5, 2, 2, hi)),
            dma((5, 2, 2, hi)),
            dma((n_tp - 1,)),
            dma((n_tp - 1,)),
            dma((n_tp - 1, bpo)),
            dma((n_tp - 1, bpo)),
            dma((n_tp - 1,)),
            dma((n_tp - 1,)),
            dma((n,)),
            dma((n_tp - 1, bpo)),
            dma((5,)),
        ],
        compiler_params=pltpu.CompilerParams(
            collective_id=0, has_side_effects=True, vmem_limit_bytes=67043328
        ),
        name="layer",
    )(
        tokens.reshape(rows, own), mix_gain.reshape(1, width), ffn_gain.reshape(1, width),
        in_scale, mix_taps, uscale, ftaps, *weights,
    )
    return result.reshape(seqs, length, own)


def solution(mesh):
    in_specs = (
        P("fs", None, "tp"),
        P(),
        P("fs", "tp"),
        P("fs", "tp"),
        P("fs", "tp"),
        P(None, "tp"),
        P(None, "tp"),
        P("tp", "fs"),
        P(None, "fs"),
        P(),
        P("fs", "tp"),
        P("fs", "tp"),
        P(None, "tp"),
        P(None, None, "tp"),
        P("tp", "fs"),
        P(None, "fs"),
    )
    out_specs = P("fs", None, "tp")
    body = functools.partial(on_device, mesh.shape["fs"], mesh.shape["tp"])
    return jax.shard_map(body, mesh=mesh, in_specs=in_specs, out_specs=out_specs, check_vma=False)
```

time: 649 us -> 294 us (0.45)
  waiting for transfers between devices: 529 us -> 0 us
  Pallas kernels: 0 us -> 277 us
  matrix products: 44 us -> 0 us
  blocking collectives: 34.1 us -> 0 us
  other arithmetic: 23.4 us -> 5.38 us
  between operations: 13.4 us -> 0.14 us
  local copies, waits for them, and re-layouts: 0.89 us -> 10.8 us
    all_gather x9 -> x0, waiting for transfers between devices: 457 us -> none  [the longest x1 90.1 us: on_device(): lax.all_gather(upgate_rows, 'fs', axis=0, tiled=True)]
    pallas_call x0 -> x1, Pallas kernels: none -> 277 us  [on_device(): pl.pallas_call(functools.partial(layer_kernel, n, n_tp, seqs), out_shape=...]
    reduce_scatter x2 -> x0, waiting for transfers between devices: 71.2 us -> none  [the longest x1 35.6 us: on_device(): lax.psum_scatter(down_terms.astype(jnp.float32).astype(jnp.bfloat16), 'tp...]
    dot_general x7 -> x0, matrix products: 44 us -> none  [the longest x5 29.8 us: dot_rows(): return jnp.dot(inputs, matrix, preferred_element_type=jnp.float32)]
    all_gather x2 -> x0, blocking collectives: 34.1 us -> none  [the longest x1 17.1 us: on_device(): lax.all_gather(mixout_scale, 'fs', axis=1, tiled=True)]
    convert_element_type x13 -> x5, other arithmetic: 18 us -> 2.83 us  [the longest x3 1.14 us: on_device(): w.astype(BF16)]
  transfers between devices with their start and end apart: 11 -> 0, of which waited for: 11 -> 0; matrix products, arithmetic and copies ran while one was open for 8% -> 0% of each run, Pallas kernels for 0% -> 0%
where the time goes in v1:
time: 294 us
  Pallas kernels  277 us (94%)
  local copies, waits for them, and re-layouts  10.8 us (4%)
  other arithmetic  5.38 us (2%)
    pallas_call x1, Pallas kernels, on_device(): pl.pallas_call(functools.partial(layer_kernel, n, n_tp, seqs), out_shape=...  277 us

profile of v1, /device:TPU:3, one launch (start us, length us, event | category | flops | bytes accessed | tf_op | source)
XLA Modules:
  0.0 293.8 jit_solution(17436179423898339636)
XLA Ops:
  0.0 0.0 copy-start.3
  0.0 0.0 copy-start.2
  0.0 0.1 pad.7.clone
  0.1 1.5 maximum_maximum_fusion.w_s
  1.6 0.8 slice_reduce_fusion.3
  2.4 0.6 copy.23
  3.0 0.9 slice_reduce_fusion.1
  4.0 0.7 reshape.27.ftaps
  4.7 1.1 convert_element_type.21
  5.7 0.0 copy-done.2
  5.8 0.0 copy-start.4
  5.8 0.0 copy-done.3
  5.8 0.0 copy-start
  5.9 0.9 pad_maximum_fusion.1.w_a
  6.8 0.0 copy-done.4
  6.8 0.8 convert_element_type.24.w_b
  7.6 0.0 copy-done
  7.6 0.3 copy.25
  7.9 1.6 copy.26
  9.5 0.1 pad_maximum_fusion
  9.6 2.1 copy.27
  11.7 0.0 copy-start.1
  11.7 1.5 reshape.28.w_c
  13.2 0.1 copy-done.1
  13.4 0.9 convert_element_type.27.w_d
  14.3 277.5 %layer.1 = bf16[768,512]{1,0:T(8,128)(2,1)} custom-call(bf16[768,512]{1,0:T(8,128)(2,1)} %bitcast.12, f32[1,2048]{1,0:T(1,128)} %bitcast.16, f32[1,2048]{1,0:T(1,128)} %bitcast.17, f32[3,512]{1,0:T(4,128)} %iscale.1, f32[3,512]{1,0:T(4,128)} %mtaps.1, f32[1,2816]{1,0:T(1,128)} %bitcast.13, f32[3,2816]{1,0:T(4,128)} %reshape.27.ftaps, ...), custom_call_target="tpu_custom_call" | custom-call | tf_op jit(solution)/shard_map/layer/pallas_call | solution.py:353
  291.8 2.1 copy.29
  (8 shorter events, 0.1 us)
Async XLA Ops:
  0.0 5.8 %copy-start.3 = (f32[256,512]{1,0:T(8,128)S(1)}, f32[256,512]{1,0:T(8,128)}, u32[]{:S(2)}) copy-start(f32[256,512]{1,0:T(8,128)} %param.20) | copy-start | bytes 1572868
  0.0 5.7 %copy-start.2 = (f32[256,512]{1,0:T(8,128)S(1)}, f32[256,512]{1,0:T(8,128)}, u32[]{:S(2)}) copy-start(f32[256,512]{1,0:T(8,128)} %param.19) | copy-start | bytes 1572868
  5.8 1.1 copy-start.4
  5.8 1.8 copy-start
  11.7 1.6 copy-start.1

commit v2 on v1

--- a/solution.py
+++ b/solution.py
@@ -24,8 +24,10 @@
 
 
 def layer_kernel(
-    n, n_tp, seqs, tok, gain1, gain2, iscale, mtaps, uscale, ftaps, w_s, w_a, w_b, w_c, w_d, out,
-    buf_s, buf_a, buf_b, buf_c, buf_d, xg, rg, normed, gated, active,
+    n, n_tp, seqs, tok, gain1, gain2, iscale, mtaps, uscale, ftaps, mscale, dscale,
+    w_bgate, w_cgate, w_value, w_mixout, w_upgate, w_upval, w_down, out,
+    buf_s, buf_a, buf_b, buf_c, buf_d, f_bgate, f_cgate, f_value, f_mixout, f_upgate, f_upval,
+    f_down, xg, rg, normed, gated, active,
     parts_m, recv_m, parts_d, recv_d,
     ring_send, ring_recv, tok_send, tok_recv, mix_send, mix_recv, res_send, res_recv,
     down_send, down_recv, local_sem,
@@ -36,7 +38,6 @@
     bpo = n // n_tp
     bw = own // bpo
     width = own * n_tp
-    weights = (w_s, w_a, w_b, w_c, w_d)
     bufs = (buf_s, buf_a, buf_b, buf_c, buf_d)
     hi, lo = n // 2, n - 1 - n // 2
 
@@ -54,12 +55,11 @@
     def ring(g, h, d, k):
         sign = 1 - 2 * d
         owner = member(pos - sign * (k - 1))
-        half = weights[g].shape[0] // 2
-        part = pl.ds(h * half, half)
-        dst = bufs[g].at[owner, part]
+        half = bufs[g].shape[1] // 2
+        piece = bufs[g].at[owner, pl.ds(h * half, half)]
         return pltpu.make_async_remote_copy(
-            src_ref=weights[g].at[part] if k == 1 else dst,
-            dst_ref=dst,
+            src_ref=piece,
+            dst_ref=piece,
             send_sem=ring_send.at[g, h, d, k - 1],
             recv_sem=ring_recv.at[g, h, d, k - 1],
             device_id={"fs": member(pos + sign)},
@@ -84,6 +84,52 @@
             src_ref=src, dst_ref=dst, send_sem=send, recv_sem=recv,
             device_id={"tp": (me + r) % n_tp}, device_id_type=MESH,
         )
+
+    sources = (w_bgate, w_cgate, w_value, w_mixout, w_upgate, w_upval, w_down)
+    floats = (f_bgate, f_cgate, f_value, f_mixout, f_upgate, f_upval, f_down)
+    loads = [
+        pltpu.make_async_copy(source, held, local_sem.at[i])
+        for i, (source, held) in enumerate(zip(sources, floats))
+    ]
+    for copy in loads:
+        copy.start()
+
+    def cast_rows(held, put):
+        tile = 32
+
+        def step(i, carry):
+            at = pl.ds(pl.multiple_of(i * tile, tile), tile)
+            put(at, held[at, :].astype(BF16))
+            return carry
+
+        lax.fori_loop(0, held.shape[0] // tile, step, 0)
+
+    def put_in(i):
+        def put(at, values):
+            buf_a[fs, at, i * own : (i + 1) * own] = values
+
+        return put
+
+    def put_up(i):
+        def put(at, values):
+            for j in range(values.shape[1] // 128):
+                to = j * 256 + i * 128
+                buf_c[fs, at, to : to + 128] = values[:, j * 128 : (j + 1) * 128]
+
+        return put
+
+    def put_mixout(at, values):
+        buf_b[fs, at, :] = values
+
+    def put_down(at, values):
+        buf_d[fs, at, :] = values
+
+    buf_s[fs] = jnp.zeros(buf_s.shape[1:], F32)
+    buf_s[fs, 0:1, :] = mscale[...]
+    buf_s[fs, 1:2, :] = dscale[...]
+    for i in range(3):
+        loads[i].wait()
+        cast_rows(floats[i], put_in(i))
 
     barrier = pltpu.get_barrier_semaphore()
     for sign in (1, -1):
@@ -103,12 +149,12 @@
     ]
     for copy in tok_copies:
         copy.start()
-    locals_ = [
-        pltpu.make_async_copy(weights[g], bufs[g].at[fs], local_sem.at[g]) for g in range(5)
-    ]
-    for copy in locals_:
-        copy.start()
     xg[me] = tok[...]
+    for copy in loads[3:]:
+        copy.wait()
+    cast_rows(f_mixout, put_mixout)
+    cast_rows(f_upgate, put_up(0))
+    cast_rows(f_upval, put_up(1))
 
     def normalize(source, gain):
         tile = 32
@@ -130,6 +176,7 @@
 
     arrive(S, 1)
     arrive(A, 1)
+    cast_rows(f_down, put_down)
     for k in range(2, hi + 1):
         arrive(S, k)
     for k in range(2, hi):
@@ -140,8 +187,6 @@
         copy.wait_recv()
     normalize(xg, gain1)
     arrive(A, hi)
-    for copy in locals_:
-        copy.wait()
 
     mixed = min(256, own)
 
@@ -232,10 +277,10 @@
         def step(j, carry):
             at = pl.ds(pl.multiple_of(j * 256, 256), 256)
             matrix = buf_c[:, :, at].reshape(width, 256)
-            both = jnp.dot(normed[lines, :], matrix, preferred_element_type=F32) * uscale[:, at]
-            both = causal_taps(both, ftaps[:, at])
-            gate, val = both[:, :128], both[:, 128:]
+            both = jnp.dot(normed[lines, :], matrix, preferred_element_type=F32)
             half = pl.ds(pl.multiple_of(j * 128, 128), 128)
+            gate = causal_taps(both[:, :128] * uscale[0:1, half], ftaps[0, :, half])
+            val = causal_taps(both[:, 128:] * uscale[1:2, half], ftaps[1, :, half])
             active[lines, half] = (gate / (1.0 + jnp.exp(-gate)) * val).astype(BF16)
             return carry
 
@@ -255,36 +300,35 @@
             part = jnp.dot(active[lines, :], buf_d[owner], preferred_element_type=F32)
             parts_d[owner, lines, :] = (part * buf_s[owner, 1:2, :]).astype(BF16)
 
-        @pl.when(r != 0)
-        def _():
-            pltpu.make_async_remote_copy(
-                src_ref=parts_d.at[owner], dst_ref=recv_d.at[r - 1, b],
-                send_sem=down_send.at[owner], recv_sem=down_recv.at[r - 1, b],
-                device_id={"tp": t}, device_id_type=MESH,
-            ).start()
-
+            @pl.when(r != 0)
+            def _():
+                pltpu.make_async_remote_copy(
+                    src_ref=parts_d.at[owner, lines], dst_ref=recv_d.at[r - 1, b, lines],
+                    send_sem=down_send.at[owner, s], recv_sem=down_recv.at[r - 1, b, s],
+                    device_id={"tp": t}, device_id_type=MESH,
+                ).start()
+
+    arrive(D, 2)
     down(fs)
     for k in range(1, hi + 1):
-        if k > 1:
+        if k > 2:
             arrive(D, k)
-        if k == 1:
-            down(member(pos - 1))
-            down(member(pos + 1))
-        elif k > 1:
-            down(member(pos - k))
-            if (2 * k) % n:
-                down(member(pos + k))
+        down(member(pos - k))
+        if (2 * k) % n:
+            down(member(pos + k))
 
     ends = []
     for r in range(1, n_tp):
         for b in range(bpo):
             owner = (me + r) % n_tp * bpo + b
-            ends.append(
-                to_peer(
-                    parts_d.at[owner], recv_d.at[r - 1, b],
-                    down_send.at[owner], down_recv.at[r - 1, b], r,
+            for s in range(seqs):
+                lines = slice(s * length, (s + 1) * length)
+                ends.append(
+                    to_peer(
+                        parts_d.at[owner, lines], recv_d.at[r - 1, b, lines],
+                        down_send.at[owner, s], down_recv.at[r - 1, b, s], r,
+                    )
                 )
-            )
     for copy in ends:
         copy.wait_recv()
 
@@ -332,31 +376,27 @@
     ff = w_upgate.shape[1]
     pad = -ff % 128
     ffp = ff + pad
-    tiles = ffp // 128
     bw = w_mixout.shape[1]
 
-    def interleaved(gate, val):
-        pair = [jnp.pad(x, ((0, 0), (0, pad))).reshape(x.shape[0], tiles, 128) for x in (gate, val)]
-        return jnp.stack(pair, axis=2).reshape(gate.shape[0], tiles * 256)
-
-    w_s = jnp.concatenate([mixout_scale, down_scale, jnp.zeros((14, bw), F32)], axis=0)
-    w_a = jnp.concatenate([w.astype(BF16) for w in (w_bgate, w_cgate, w_value)], axis=1)
-    w_b = w_mixout.astype(BF16)
-    w_c = interleaved(w_upgate.astype(BF16), w_upval.astype(BF16))
-    w_d = jnp.pad(w_down.astype(BF16), ((0, pad), (0, 0)))
-    uscale = interleaved(up_scale[0:1], up_scale[1:2])
-    ftaps = interleaved(ffn_taps[0], ffn_taps[1])
-    weights = (w_s, w_a, w_b, w_c, w_d)
+    if pad:
+        w_upgate, w_upval, up_scale, ffn_taps = (
+            jnp.pad(x, [(0, 0)] * (x.ndim - 1) + [(0, pad)])
+            for x in (w_upgate, w_upval, up_scale, ffn_taps)
+        )
+        w_down = jnp.pad(w_down, ((0, pad), (0, 0)))
+    weights = (w_bgate, w_cgate, w_value, w_mixout, w_upgate, w_upval, w_down)
+    held = [(16, bw), (part, 3 * own), w_mixout.shape, (part, 2 * ffp), w_down.shape]
     bpo = n // n_tp
     hi = n // 2
     vmem, dma = pltpu.VMEM, pltpu.SemaphoreType.DMA
     result = pl.pallas_call(
         functools.partial(layer_kernel, n, n_tp, seqs),
         out_shape=jax.ShapeDtypeStruct((rows, own), BF16),
-        in_specs=[pl.BlockSpec(memory_space=pltpu.VMEM)] * 7
-        + [pl.BlockSpec(memory_space=pl.ANY)] * 5,
+        in_specs=[pl.BlockSpec(memory_space=pltpu.VMEM)] * 9
+        + [pl.BlockSpec(memory_space=pl.ANY)] * 7,
         out_specs=pl.BlockSpec(memory_space=pltpu.VMEM),
-        scratch_shapes=[vmem((n, *w.shape), w.dtype) for w in weights]
+        scratch_shapes=[vmem((n, *shape), BF16 if i else F32) for i, shape in enumerate(held)]
+        + [vmem(w.shape, F32) for w in weights]
         + [
             vmem((n_tp, rows, own), BF16),
             vmem((n_tp, rows, own), BF16),
@@ -375,9 +415,9 @@
             dma((n_tp - 1, bpo)),
             dma((n_tp - 1,)),
             dma((n_tp - 1,)),
-            dma((n,)),
-            dma((n_tp - 1, bpo)),
-            dma((5,)),
+            dma((n, seqs)),
+            dma((n_tp - 1, bpo, seqs)),
+            dma((7,)),
         ],
         compiler_params=pltpu.CompilerParams(
             collective_id=0, has_side_effects=True, vmem_limit_bytes=67043328
@@ -385,7 +425,7 @@
         name="layer",
     )(
         tokens.reshape(rows, own), mix_gain.reshape(1, width), ffn_gain.reshape(1, width),
-        in_scale, mix_taps, uscale, ftaps, *weights,
+        in_scale, mix_taps, up_scale, ffn_taps, mixout_scale, down_scale, *weights,
     )
     return result.reshape(seqs, length, own)
 

time: 294 us -> 283 us (0.963)
  local copies, waits for them, and re-layouts: 10.8 us -> 3.45 us
  other arithmetic: 5.38 us -> 0 us
where the time goes in v2:
time: 283 us; the launch traced here: 282 us
  Pallas kernels  279 us (99%)
  local copies, waits for them, and re-layouts  3.45 us (1%)
    pallas_call x1, Pallas kernels, on_device(): pl.pallas_call(functools.partial(layer_kernel, n, n_tp, seqs), out_shape=...  279 us

profile of v2, /device:TPU:3, one launch (start us, length us, event | category | flops | bytes accessed | tf_op | source)
XLA Modules:
  0.0 282.5 jit_solution(10848907504932910722)
XLA Ops:
  0.0 1.4 copy.17.ftaps
  1.4 279.0 %layer.1 = bf16[768,512]{1,0:T(8,128)(2,1)} custom-call(bf16[768,512]{1,0:T(8,128)(2,1)} %bitcast.5, f32[1,2048]{1,0:T(1,128)} %bitcast.6, f32[1,2048]{1,0:T(1,128)} %bitcast.7, f32[3,512]{1,0:T(4,128)} %iscale.1, f32[3,512]{1,0:T(4,128)} %mtaps.1, f32[2,1408]{1,0:T(2,128)} %uscale.1, f32[2,3,1408]{2,1,0:T(4,128)} %copy.17.ftaps, f32[1,256]{1,0:T(1,128)} %mscale.1, ...), custom_call_target="tpu_custom_call" | custom-call | tf_op jit(solution)/shard_map/layer/pallas_call | solution.py:392
  280.4 2.1 copy.19

commit v3 on v2

--- a/solution.py
+++ b/solution.py
@@ -213,8 +213,11 @@
         if s == 0:
             arrive(B, 1)
     begin(C, (1,))
-    for k in range(2, hi + 1):
+    for k in range(2, hi):
         arrive(B, k)
+    arrive(C, 1, (0,))
+    arrive(B, hi)
+    arrive(C, 1, (1,))
 
     mix_copies = []
     for r in list(range(1, n_tp)) + [0]:
@@ -231,7 +234,7 @@
                 )
                 copy.start()
                 mix_copies.append(copy)
-    arrive(C, 1)
+    arrive(C, 2, (0,))
 
     for copy in mix_copies:
         copy.wait_recv()
@@ -260,12 +263,12 @@
     ]
     for copy in res_copies:
         copy.start()
-    arrive(C, 2)
+    arrive(C, 2, (1,))
     for k in range(3, hi):
         arrive(C, k)
+    begin(D)
     for copy in res_copies:
         copy.wait_recv()
-    begin(D)
     normalize(rg, gain2)
     arrive(C, hi)
 

time: 283 us -> 280 us (0.989)
  Pallas kernels: 279 us -> 276 us
    pallas_call x1, Pallas kernels: 279 us -> 276 us  [on_device(): pl.pallas_call(functools.partial(layer_kernel, n, n_tp, seqs), out_shape=...]
where the time goes in v3:
time: 280 us; the launch traced here: 279 us
  Pallas kernels  276 us (99%)
  local copies, waits for them, and re-layouts  3.45 us (1%)
    pallas_call x1, Pallas kernels, on_device(): pl.pallas_call(functools.partial(layer_kernel, n, n_tp, seqs), out_shape=...  276 us

profile of v3, /device:TPU:3, one launch (start us, length us, event | category | flops | bytes accessed | tf_op | source)
XLA Modules:
  0.0 279.3 jit_solution(1873455611510781969)
XLA Ops:
  0.0 1.4 copy.17.ftaps
  1.4 275.8 %layer.1 = bf16[768,512]{1,0:T(8,128)(2,1)} custom-call(bf16[768,512]{1,0:T(8,128)(2,1)} %bitcast.5, f32[1,2048]{1,0:T(1,128)} %bitcast.6, f32[1,2048]{1,0:T(1,128)} %bitcast.7, f32[3,512]{1,0:T(4,128)} %iscale.1, f32[3,512]{1,0:T(4,128)} %mtaps.1, f32[2,1408]{1,0:T(2,128)} %uscale.1, f32[2,3,1408]{2,1,0:T(4,128)} %copy.17.ftaps, f32[1,256]{1,0:T(1,128)} %mscale.1, ...), custom_call_target="tpu_custom_call" | custom-call | tf_op jit(solution)/shard_map/layer/pallas_call | solution.py:395
  277.2 2.1 copy.19
